TPU v7x, 256 devices: a 4x2x16 block of a 4x16x16 slice. The times are simulated.
256 devices in a mesh: grp: 2 (over y), fs: 16 (over z), tp: 8 (over x, core).
Axes of the slice: x: 4, y: 2, z: 16, core: 2. Of those that a mesh axis runs over, the one named last changes fastest.
The devices are a block of a 4x16x16 slice.
Arguments:
- tokens: bfloat16 [32768, 2048], P(('grp', 'fs')), parts along dimension 0, may hold values from -1300 to 1300
- norm_gain: bfloat16 [2048], replicated, may hold values from 0.099609375 to 1.8984375
- gate_weight: bfloat16 [2048, 5120], P('fs', 'tp'), may hold values from -0.125 to 0.125
- up_weight: bfloat16 [2048, 5120], P('fs', 'tp'), may hold values from -0.125 to 0.125
- down_weight: bfloat16 [5120, 2048], P('tp', 'fs'), may hold values from -0.078125 to 0.078125
Outputs:
- mixed: bfloat16 [32768, 2048], P(('grp', 'fs', 'tp')), parts along dimension 0
There are 2 independent parts, one for each index of `grp`. A program takes and returns all parts, laid end to end along the dimension named above; an argument that names none is the same for every part. Nothing has to cross between parts.
All inputs are finite; a program needn't handle non-finite values.
Results may differ from a plain program's by a relative error of at most 0.013.
Values may be sent and summed in bfloat16 or wider, within the bound.
No kernel may reach another device: no remote copies, remote signals or barrier semaphores. Data moves between devices by JAX's collectives and lax.ppermute only.
A program may use at most 64 MiB of HBM per device.

v0:
```python
import jax
import jax.numpy as jnp
from jax import lax
from jax.sharding import PartitionSpec as P

EPSILON = 1e-06


def side_by_side(arrays, axis, dim, along):
    widths = [a.shape[along] for a in arrays]
    both = jnp.concatenate(arrays, axis=along)
    result = lax.all_gather(both, axis, axis=dim, tiled=True)
    return tuple(jnp.split(result, [sum(widths[:k]) for k in range(1, len(widths))], axis=along))


def normalize(tokens, norm_gain):
    as_float = tokens.astype(jnp.float32)
    scale = lax.rsqrt(jnp.mean(as_float * as_float, axis=-1, keepdims=True) + EPSILON)
    return (as_float * scale * norm_gain.astype(jnp.float32)).astype(jnp.bfloat16)


def rounded(values):
    return lax.optimization_barrier(values.astype(jnp.bfloat16)).astype(jnp.float32)


def on_device(tokens, norm_gain, gate_weight, up_weight, down_weight):
    normed = normalize(tokens, norm_gain)
    down_whole = lax.all_gather(down_weight, "fs", axis=1, tiled=True)
    gate_whole, up_whole = side_by_side((gate_weight, up_weight), "fs", 0, 1)
    gate_acts = jnp.dot(normed, gate_whole, preferred_element_type=jnp.float32)
    up_acts = jnp.dot(normed, up_whole, preferred_element_type=jnp.float32)
    hidden = (jax.nn.silu(gate_acts) * up_acts).astype(jnp.bfloat16)
    return lax.psum_scatter(
        rounded(jnp.dot(hidden, down_whole, preferred_element_type=jnp.float32)).astype(
            jnp.bfloat16
        ),
        "tp",
        scatter_dimension=0,
        tiled=True,
    )


def solution(mesh):
    return jax.shard_map(
        on_device,
        mesh=mesh,
        in_specs=(P(("grp", "fs"), None), P(), P("fs", "tp"), P("fs", "tp"), P("tp", "fs")),
        out_specs=P(("grp", "fs", "tp"), None),
        check_vma=False,
    )
```

profile of v0, /device:TPU:40, one launch (start us, length us, event | category | flops | bytes accessed | tf_op | source)
XLA Modules:
  0.0 240.0 jit_solution(12156880815646767167)
XLA Ops:
  6.5 0.0 all-gather.3.cloned.1.call-start
  6.6 1.7 pad_maximum_fusion
  8.3 0.1 all-gather.3.cloned.1.call-update
  8.4 0.1 all-gather.5.cloned.1.call-start
  8.4 0.7 all-gather.5.cloned.1.call-update
  9.2 0.1 reduce-scatter.2.cloned.1.call-start
  9.2 0.7 convert_element_type.18
  9.9 3.1 %fusion = f32[1024]{0:T(1024)S(1)} fusion(bf16[1024,2048]{1,0:T(8,128)(2,1)} %param.5), kind=kLoop, calls=%fused_computation.2 | loop fusion | flops 6290432 | bytes 4198400 | tf_op jit(solution)/shard_map/reduce_sum | solution.py:18
  13.0 88.4 %all-gather.3.cloned.1.call-done = bf16[2048,1280]{1,0:T(8,128)(2,1)} async-done(((bf16[128,1280]{1,0:T(8,128)(2,1)}), bf16[2048,1280]{1,0:T(8,128)(2,1)}) %all-gather.3.cloned.1.call-update) | async-done | bytes 5242896 | tf_op jit(solution)/shard_map/all_gather | solution.py:12
  101.4 6.3 %fusion.3 = f32[1024,640]{1,0:T(8,128)S(1)} fusion(bf16[2048,1280]{1,0:T(8,128)(2,1)} %all-gather.3.cloned.1.call-done, bf16[1024,2048]{1,0:T(8,128)(2,1)} %param.5, f32[2048]{0:T(1024)S(1)} %convert_element_type.18, f32[1024]{0:T(1024)S(1)} %add_rsqrt_fusion), kind=kOutput, calls=%fused_computation.6 | convolution fusion | flops 2692743168 | bytes 9449472 | tf_op jit(solution)/shard_map/dot_general | solution.py:31
  107.7 72.3 %all-gather.5.cloned.1.call-done = bf16[640,2048]{1,0:T(8,128)(2,1)} async-done(((bf16[640,128]{1,0:T(8,128)(2,1)}), bf16[640,2048]{1,0:T(8,128)(2,1)}) %all-gather.5.cloned.1.call-update) | async-done | bytes 2621456 | tf_op jit(solution)/shard_map/all_gather | solution.py:28
  180.0 12.9 %convolution_convert_fusion = bf16[1024,2048]{1,0:T(8,128)(2,1)} fusion(bf16[640,2048]{1,0:T(8,128)(2,1)} %all-gather.5.cloned.1.call-done, f32[1024,640]{1,0:T(8,128)S(1)} %fusion.3, bf16[2048,1280]{1,0:T(8,128)(2,1)} %all-gather.3.cloned.1.call-done, bf16[1024,2048]{1,0:T(8,128)(2,1)} %param.5, f32[2048]{0:T(1024)S(1)} %convert_element_type.18, ...), kind=kOutput, calls=%fused_computation.5 | convolution fusion | flops 5383127040 | bytes 16265216 | tf_op jit(solution)/shard_map/dot_general | solution.py:34
  192.9 0.1 reduce-scatter.2.cloned.1.call-update
  192.9 40.5 %reduce-scatter.2.cloned.1.call-done = bf16[128,2048]{1,0:T(8,128)(2,1)} async-done(((bf16[1024,2048]{1,0:T(8,128)(2,1)}), bf16[128,2048]{1,0:T(8,128)(2,1)}) %reduce-scatter.2.cloned.1.call-update) | async-done | bytes 524304 | tf_op jit(solution)/shard_map/reduce_scatter | solution.py:33
  (1 shorter events, 0.0 us)
Async XLA Ops:
  6.5 94.9 %all-gather.3.cloned.1.call-start = ((), (), s32[]{:S(2)}) async-start(), calls=%async_computation.1 | async-start | bytes 5570560 | tf_op jit(solution)/shard_map/all_gather | solution.py:12
  8.4 171.7 %all-gather.5.cloned.1.call-start = ((), (), s32[]{:S(2)}) async-start(), calls=%async_computation.2 | async-start | bytes 2785280 | tf_op jit(solution)/shard_map/all_gather | solution.py:28
  9.2 224.2 %reduce-scatter.2.cloned.1.call-start = ((), (), s32[]{:S(2)}) async-start(), calls=%async_computation.3 | async-start | bytes 4718592 | tf_op jit(solution)/shard_map/reduce_scatter | solution.py:33
Sparse Core Ops, SparseCore 0:
  9.1 92.2 all-gather.2
  103.2 76.7 all-gather.4
  193.0 40.3 reduce-scatter.1
where the time goes:
time: 240 us
  waiting for transfers between devices  202 us (84%)
  matrix products  19.1 us (8%)
  between operations  13.1 us (5%)
  other arithmetic  5.51 us (2%)
    all_gather x1, waiting for transfers between devices, side_by_side(): result = lax.all_gather(both, axis, axis=dim, tiled=True)  88.4 us
    all_gather x1, waiting for transfers between devices, on_device(): down_whole = lax.all_gather(down_weight, 'fs', axis=1, tiled=True)  72.3 us
    reduce_scatter x1, waiting for transfers between devices, on_device(): lax.psum_scatter(rounded(jnp.dot(hidden, down_whole, preferred_element_ty...  40.5 us
    dot_general x1, matrix products, on_device(): jnp.dot(hidden, down_whole, preferred_element_type=jnp.float32)  12.9 us
    dot_general x1, matrix products, on_device(): up_acts = jnp.dot(normed, up_whole, preferred_element_type=jnp.float32)  6.29 us
  transfers between devices with their start and end apart: 3, of which 3 were waited for; matrix products, arithmetic and copies ran while one was open for 4% of the time, Pallas kernels for 0%

commit v1 on v0

--- a/solution.py
+++ b/solution.py
@@ -25,7 +25,9 @@
 
 def on_device(tokens, norm_gain, gate_weight, up_weight, down_weight):
     normed = normalize(tokens, norm_gain)
-    down_whole = lax.all_gather(down_weight, "fs", axis=1, tiled=True)
+    down_whole = jnp.concatenate(
+        lax.all_to_all(jnp.stack([down_weight] * lax.axis_size("fs")), "fs", 0, 0), axis=1
+    )
     gate_whole, up_whole = side_by_side((gate_weight, up_weight), "fs", 0, 1)
     gate_acts = jnp.dot(normed, gate_whole, preferred_element_type=jnp.float32)
     up_acts = jnp.dot(normed, up_whole, preferred_element_type=jnp.float32)

time: 240 us -> 278 us (1.16)
  starting transfers between devices: 0.13 us -> 24 us
  waiting for transfers between devices: 202 us -> 212 us
  local copies, waits for them, and re-layouts: 0 us -> 2.89 us
    all_gather x1, waiting for transfers between devices: 88.4 us -> 170 us  [side_by_side(): result = lax.all_gather(both, axis, axis=dim, tiled=True)]
    all_gather x1 -> x0, waiting for transfers between devices: 72.3 us -> none  [on_device(): down_whole = lax.all_gather(down_weight, 'fs', axis=1, tiled=True)]
    all_to_all x0 -> x1, starting transfers between devices: none -> 24 us  [on_device(): lax.all_to_all(jnp.stack([down_weight] * lax.axis_size('fs')), 'fs', 0, 0)]
  transfers between devices with their start and end apart: 3 -> 3, of which waited for: 3 -> 2; matrix products, arithmetic and copies ran while one was open for 4% -> 5% of each run, Pallas kernels for 0% -> 0%
where the time goes in v1:
time: 278 us; the launch traced here: 277 us
  waiting for transfers between devices  212 us (76%)
  starting transfers between devices  24 us (9%)
  matrix products  20.3 us (7%)
  between operations  13.5 us (5%)
  other arithmetic  4.87 us (2%)
  local copies, waits for them, and re-layouts  2.89 us (1%)
    all_gather x1, waiting for transfers between devices, side_by_side(): result = lax.all_gather(both, axis, axis=dim, tiled=True)  170 us
    reduce_scatter x1, waiting for transfers between devices, on_device(): lax.psum_scatter(rounded(jnp.dot(hidden, down_whole, preferred_element_ty...  41.2 us
    all_to_all x1, starting transfers between devices, on_device(): lax.all_to_all(jnp.stack([down_weight] * lax.axis_size('fs')), 'fs', 0, 0)  24 us
    dot_general x1, matrix products, on_device(): jnp.dot(hidden, down_whole, preferred_element_type=jnp.float32)  12.4 us
    dot_general x1, matrix products, on_device(): up_acts = jnp.dot(normed, up_whole, preferred_element_type=jnp.float32)  7.95 us
  transfers between devices with their start and end apart: 3, of which 2 were waited for; matrix products, arithmetic and copies ran while one was open for 5% of the time, Pallas kernels for 0%

profile of v1, /device:TPU:40, one launch (start us, length us, event | category | flops | bytes accessed | tf_op | source)
XLA Modules:
  0.0 277.4 jit_solution(13340435810106685425)
XLA Ops:
  6.5 0.0 all-gather.2.cloned.1.call-start
  6.6 1.7 pad_maximum_fusion
  8.3 0.1 all-gather.2.cloned.1.call-update
  8.4 0.0 copy-start
  8.4 1.1 copy.6
  9.4 1.8 stack.2
  11.3 24.0 %all-to-all-start = ((bf16[16,640,128]{1,2,0:T(8,128)(2,1)}), bf16[16,640,128]{1,2,0:T(8,128)(2,1)S(1)}, u32[]{:S(2)}, u32[]{:S(2)}) async-start(bf16[16,640,128]{1,2,0:T(8,128)(2,1)} %stack.2), calls=%async_computation | async-start | bytes 5242880 | tf_op jit(solution)/shard_map/all_to_all | solution.py:29
  35.2 0.1 reduce-scatter.2.cloned.1.call-start
  35.3 0.0 copy-done
  35.3 3.1 %fusion = f32[1024]{0:T(1024)S(1)} fusion(bf16[1024,2048]{1,0:T(8,128)(2,1)} %param.5), kind=kLoop, calls=%fused_computation.2 | loop fusion | flops 6290432 | bytes 4198400 | tf_op jit(solution)/shard_map/reduce_sum | solution.py:18
  38.5 170.5 %all-gather.2.cloned.1.call-done = bf16[2048,1280]{1,0:T(8,128)(2,1)} async-done(((bf16[128,1280]{1,0:T(8,128)(2,1)}), bf16[2048,1280]{1,0:T(8,128)(2,1)}) %all-gather.2.cloned.1.call-update) | async-done | bytes 5242896 | tf_op jit(solution)/shard_map/all_gather | solution.py:12
  209.0 8.0 %fusion.3 = f32[1024,640]{1,0:T(8,128)} fusion(bf16[2048,1280]{1,0:T(8,128)(2,1)} %all-gather.2.cloned.1.call-done, bf16[1024,2048]{1,0:T(8,128)(2,1)} %param.5, f32[2048]{0:T(1024)S(1)} %convert_element_type.18, f32[1024]{0:T(1024)S(1)} %add_rsqrt_fusion), kind=kOutput, calls=%fused_computation.6 | convolution fusion | flops 2692743168 | bytes 9449472 | tf_op jit(solution)/shard_map/dot_general | solution.py:33
  216.9 0.0 all-to-all-done
  216.9 12.4 %convolution_convert_fusion = bf16[1024,2048]{1,0:T(8,128)(2,1)} fusion(bf16[640,2048]{0,1:T(8,128)(2,1)S(1)} %bitcast.4, f32[1024,640]{1,0:T(8,128)} %fusion.3, bf16[2048,1280]{1,0:T(8,128)(2,1)} %all-gather.2.cloned.1.call-done, bf16[1024,2048]{1,0:T(8,128)(2,1)} %param.5, f32[2048]{0:T(1024)S(1)} %convert_element_type.18, f32[1024]{0:T(1024)S(1)} %add_rsqrt_fusion), kind=kOutput, calls=%fused_computation.5 | convolution fusion | flops 5383127040 | bytes 16265216 | tf_op jit(solution)/shard_map/dot_general | solution.py:36
  229.3 0.1 reduce-scatter.2.cloned.1.call-update
  229.4 41.2 %reduce-scatter.2.cloned.1.call-done = bf16[128,2048]{1,0:T(8,128)(2,1)} async-done(((bf16[1024,2048]{1,0:T(8,128)(2,1)}), bf16[128,2048]{1,0:T(8,128)(2,1)}) %reduce-scatter.2.cloned.1.call-update) | async-done | bytes 524304 | tf_op jit(solution)/shard_map/reduce_scatter | solution.py:35
  (2 shorter events, 0.0 us)
Async XLA Ops:
  6.5 202.4 %all-gather.2.cloned.1.call-start = ((), (), s32[]{:S(2)}) async-start(), calls=%async_computation.2 | async-start | bytes 5570560 | tf_op jit(solution)/shard_map/all_gather | solution.py:12
  8.4 27.0 %copy-start = (bf16[2048]{0:T(1024)(128)(2,1)S(1)}, bf16[2048]{0:T(1024)(128)(2,1)}, u32[]{:S(2)}) copy-start(bf16[2048]{0:T(1024)(128)(2,1)} %param.6) | copy-start | bytes 12292
  11.3 205.7 %all-to-all-start = ((bf16[16,640,128]{1,2,0:T(8,128)(2,1)}), bf16[16,640,128]{1,2,0:T(8,128)(2,1)S(1)}, u32[]{:S(2)}, u32[]{:S(2)}) async-start(bf16[16,640,128]{1,2,0:T(8,128)(2,1)} %stack.2), calls=%async_computation | async-start | bytes 5242880 | tf_op jit(solution)/shard_map/all_to_all | solution.py:29
  35.2 235.3 %reduce-scatter.2.cloned.1.call-start = ((), (), s32[]{:S(2)}) async-start(), calls=%async_computation.3 | async-start | bytes 4718592 | tf_op jit(solution)/shard_map/reduce_scatter | solution.py:35
Sparse Core Ops, SparseCore 0:
  9.1 199.7 all-gather.1
  229.5 40.9 reduce-scatter.1
